TPU v7x, 32 devices: a whole 2x2x4 slice. The times are simulated.
32 devices in a mesh: fs: 4 (over z), rep: 4 (over y, x), tp: 2 (over core).
Axes of the slice: x: 2, y: 2, z: 4, core: 2. Of those that a mesh axis runs over, the one named last changes fastest.
Arguments:
- query_input: bfloat16 [16384, 4096], P(('fs', 'rep')), may hold values from -6 to 6
- query_cotangent: bfloat16 [16384, 1024], P(('fs', 'rep'), 'tp'), may hold values from -0.046875 to 0.046875
- branch_output: bfloat16 [16384, 2048], P(('fs', 'rep')), may hold values from -6 to 6
- layer_cotangent: bfloat16 [16384, 4096], P(('fs', 'rep'), 'tp'), may hold values from -0.046875 to 0.046875
- query_weight: float32 [4096, 1024], P(('rep', 'fs'), 'tp'), may hold values from -0.09375 to 0.09375
- output_weight: float32 [2048, 4096], P(('rep', 'fs'), 'tp'), may hold values from -0.125 to 0.125
- query_basis: bfloat16 [4096, 512], P(('rep', 'fs')), may hold values from -0.09375 to 0.09375
- output_basis: bfloat16 [2048, 512], P(('rep', 'fs')), may hold values from -0.125 to 0.125
- query_first: float32 [512, 1024], P(('rep', 'fs'), 'tp'), may hold values from -20 to 20
- query_second: float32 [512, 1024], P(('rep', 'fs'), 'tp'), may hold values from 0.25 to 2
- output_first: float32 [512, 4096], P(('rep', 'fs'), 'tp'), may hold values from -20 to 20
- output_second: float32 [512, 4096], P(('rep', 'fs'), 'tp'), may hold values from 0.25 to 2
Outputs:
- query_update: float32 [4096, 1024], P(('rep', 'fs'), 'tp')
- output_update: float32 [2048, 4096], P(('rep', 'fs'), 'tp')
- query_first_next: float32 [512, 1024], P(('rep', 'fs'), 'tp')
- query_second_next: float32 [512, 1024], P(('rep', 'fs'), 'tp')
- output_first_next: float32 [512, 4096], P(('rep', 'fs'), 'tp')
- output_second_next: float32 [512, 4096], P(('rep', 'fs'), 'tp')
- query_copy: bfloat16 [4096, 1024], P('rep', 'tp')
- output_copy: bfloat16 [2048, 4096], P('rep', 'tp')
All inputs are finite; a program needn't handle non-finite values.
Results may differ from a plain program's by a relative error of at most 0.0055.
Values may be sent and summed in bfloat16 or wider, within the bound.
A program may use at most 128 MiB of HBM per device.

v0:
```python
import jax
import jax.numpy as jnp
from jax import lax
from jax.sharding import PartitionSpec as P

D = 4096
QKW = 1024
R = 512
beta_first = 0.6
beta_second = 0.8
step_rate = 0.01
small_eps = 1e-06


def split_parts(values):
    upper = values.astype(jnp.bfloat16)
    lower = (values - upper.astype(jnp.float32)).astype(jnp.bfloat16)
    return (upper, lower)


def split_rows(inner, cotangent):
    upper, lower = split_parts(inner)
    dims = (((0,), (0,)), ((), ()))
    return lax.dot_general(
        upper, cotangent, dims, preferred_element_type=jnp.float32
    ) + lax.dot_general(lower, cotangent, dims, preferred_element_type=jnp.float32)


def moments(first, second, projected):
    first_next = beta_first * first + (1.0 - beta_first) * projected
    second_next = beta_second * second + (1.0 - beta_second) * projected * projected
    return (first_next, second_next, first_next / jnp.sqrt(second_next))


def body(
    query_input,
    query_cotangent,
    branch_output,
    layer_cotangent,
    query_weight,
    output_weight,
    query_basis,
    output_basis,
    query_first,
    query_second,
    output_first,
    output_second,
):
    query_whole, output_whole = (
        lax.all_gather(query_basis, ("rep", "fs"), axis=0, tiled=True),
        lax.all_gather(output_basis, ("rep", "fs"), axis=0, tiled=True),
    )
    query_inner = jnp.dot(query_input, query_whole, preferred_element_type=jnp.float32)
    output_inner = jnp.dot(branch_output, output_whole, preferred_element_type=jnp.float32)
    projected_q = lax.psum_scatter(
        split_rows(query_inner, query_cotangent), ("rep", "fs"), scatter_dimension=0, tiled=True
    )
    projected_o = lax.psum_scatter(
        split_rows(output_inner, layer_cotangent), ("rep", "fs"), scatter_dimension=0, tiled=True
    )
    first_q, second_q, normed_q = moments(query_first, query_second, projected_q)
    first_o, second_o, normed_o = moments(output_first, output_second, projected_o)
    totals = lax.psum(
        (jnp.sum(normed_q * normed_q), jnp.sum(normed_o * normed_o)), ("fs", "rep", "tp")
    )
    scale_q = lax.rsqrt(totals[0] / (R * QKW) + small_eps)
    scale_o = lax.rsqrt(totals[1] / (R * D) + small_eps)
    summed_q = jnp.dot(
        query_basis,
        lax.all_gather(normed_q.astype(jnp.bfloat16), ("rep", "fs"), axis=0, tiled=True),
        preferred_element_type=jnp.float32,
    )
    summed_o = jnp.dot(
        output_basis,
        lax.all_gather(normed_o.astype(jnp.bfloat16), ("rep", "fs"), axis=0, tiled=True),
        preferred_element_type=jnp.float32,
    )
    update_q = scale_q * summed_q
    update_o = scale_o * summed_o
    query_copy, output_copy = (
        lax.all_gather(
            (query_weight - step_rate * update_q).astype(jnp.bfloat16), "fs", axis=0, tiled=True
        ),
        lax.all_gather(
            (output_weight - step_rate * update_o).astype(jnp.bfloat16), "fs", axis=0, tiled=True
        ),
    )
    return (update_q, update_o, first_q, second_q, first_o, second_o, query_copy, output_copy)


def solution(mesh):
    in_specs = (
        P(("fs", "rep"), None),
        P(("fs", "rep"), "tp"),
        P(("fs", "rep"), None),
        P(("fs", "rep"), "tp"),
        P(("rep", "fs"), "tp"),
        P(("rep", "fs"), "tp"),
        P(("rep", "fs"), None),
        P(("rep", "fs"), None),
        P(("rep", "fs"), "tp"),
        P(("rep", "fs"), "tp"),
        P(("rep", "fs"), "tp"),
        P(("rep", "fs"), "tp"),
    )
    out_specs = (
        P(("rep", "fs"), "tp"),
        P(("rep", "fs"), "tp"),
        P(("rep", "fs"), "tp"),
        P(("rep", "fs"), "tp"),
        P(("rep", "fs"), "tp"),
        P(("rep", "fs"), "tp"),
        P("rep", "tp"),
        P("rep", "tp"),
    )
    return jax.shard_map(body, mesh=mesh, in_specs=in_specs, out_specs=out_specs, check_vma=False)
```

profile of v0, /device:TPU:0, one launch (start us, length us, event | category | flops | bytes accessed | tf_op | source)
XLA Modules:
  0.0 505.3 jit_solution(10517695907345015072)
XLA Ops:
  8.0 0.7 all-gather.6.cloned.1.call-update
  8.7 65.3 %all-gather.8.cloned.1.call-done = bf16[2048,512]{1,0:T(8,128)(2,1)} async-done(((bf16[128,512]{1,0:T(8,128)(2,1)}), bf16[2048,512]{1,0:T(8,128)(2,1)}) %all-gather.8.cloned.1.call-update) | async-done | bytes 2097168 | tf_op jit(solution)/shard_map/all_gather | solution.py:51
  74.0 5.3 %fusion.15 = f32[1024,512]{1,0:T(8,128)S(1)} fusion(bf16[1024,2048]{1,0:T(8,128)(2,1)} %param.14, bf16[2048,512]{1,0:T(8,128)(2,1)} %all-gather.8.cloned.1.call-done), kind=kOutput, calls=%fused_computation.29 | convolution fusion | flops 2147483648 | bytes 8388608 | tf_op jit(solution)/shard_map/dot_general | solution.py:54
  79.4 2.4 fusion.3
  81.7 4.4 convolution_add_fusion
  86.2 65.0 %all-gather.6.cloned.1.call-done = bf16[4096,512]{1,0:T(8,128)(2,1)} async-done(((bf16[256,512]{1,0:T(8,128)(2,1)}), bf16[4096,512]{1,0:T(8,128)(2,1)}) %all-gather.6.cloned.1.call-update) | async-done | bytes 4194320 | tf_op jit(solution)/shard_map/all_gather | solution.py:50
  151.2 8.1 %fusion.14 = f32[1024,512]{1,0:T(8,128)S(1)} fusion(bf16[1024,4096]{1,0:T(8,128)(2,1)} %param.12, bf16[4096,512]{1,0:T(8,128)(2,1)} %all-gather.6.cloned.1.call-done), kind=kOutput, calls=%fused_computation.28 | convolution fusion | flops 4294967296 | bytes 14680064 | tf_op jit(solution)/shard_map/dot_general | solution.py:53
  159.3 0.7 fusion.6
  160.1 1.7 convolution_add_fusion.1
  161.9 87.6 %reduce-scatter.5.cloned.1.call-done = f32[32,2048]{1,0:T(8,128)} async-done(((f32[512,2048]{1,0:T(8,128)}), f32[32,2048]{1,0:T(8,128)}) %reduce-scatter.5.cloned.1.call-update) | async-done | bytes 262160 | tf_op jit(solution)/shard_map/reduce_scatter | solution.py:58
  249.6 1.7 fusion.9
  251.5 79.1 %reduce-scatter.3.cloned.1.call-done = f32[32,512]{1,0:T(8,128)} async-done(((f32[512,512]{1,0:T(8,128)}), f32[32,512]{1,0:T(8,128)}) %reduce-scatter.3.cloned.1.call-update) | async-done | bytes 65552 | tf_op jit(solution)/shard_map/reduce_scatter | solution.py:55
  330.6 1.5 multiply_reduce_fusion.1
  332.8 43.2 %all_gather.19 = bf16[512,512]{1,0:T(8,128)(2,1)S(1)} all-gather(bf16[32,512]{1,0:T(8,128)(2,1)S(1)} %fusion.11), channel_id=1, replica_groups=mesh['fs'=4,'rep'=4,'tp'=2] {'rep','fs'}, dimensions={0}, use_global_device_ids=true | all-gather | bytes 557056 | tf_op jit(solution)/shard_map/all_gather | solution.py:70
  376.7 37.8 %all-reduce = (f32[]{:T(128)}, f32[]{:T(128)}) all-reduce(f32[]{:T(128)} %get-tuple-element.21, f32[]{:T(128)} %multiply_reduce_fusion), channel_id=1, replica_groups=mesh['fs'=4,'rep'=4,'tp'=2] {'fs','rep','tp'}, use_global_device_ids=true, to_apply=%region_2.0 | all-reduce | flops 2 | bytes 16 | tf_op jit(solution)/shard_map/psum | solution.py:63
  415.2 1.2 subtract_convert_fusion.5
  416.5 1.6 copy.21
  418.8 3.1 subtract_convert_fusion.4
  421.9 2.0 copy.22
  424.0 23.8 %all-gather.12.cloned.1.call-done = bf16[1024,512]{0,1:T(8,128)(2,1)} async-done(((bf16[256,512]{0,1:T(8,128)(2,1)}), bf16[1024,512]{0,1:T(8,128)(2,1)}) %all-gather.12.cloned.1.call-update) | async-done | bytes 1048592 | tf_op jit(solution)/shard_map/all_gather | solution.py:81
  447.8 2.3 copy.24
  450.1 1.3 copy.23
  451.4 43.1 %all-gather.14.cloned.1.call-done = bf16[512,2048]{0,1:T(8,128)(2,1)} async-done(((bf16[128,2048]{0,1:T(8,128)(2,1)}), bf16[512,2048]{0,1:T(8,128)(2,1)}) %all-gather.14.cloned.1.call-update) | async-done | bytes 2097168 | tf_op jit(solution)/shard_map/all_gather | solution.py:84
  494.5 3.9 copy.25
  (43 shorter events, 2.7 us)
Async XLA Ops:
  7.2 152.2 %copy-start = (bf16[1024,512]{1,0:T(8,128)(2,1)S(1)}, bf16[1024,512]{1,0:T(8,128)(2,1)}, u32[]{:S(2)}) copy-start(bf16[1024,512]{1,0:T(8,128)(2,1)} %param.13) | copy-start | bytes 3145732
  7.2 66.8 %all-gather.8.cloned.1.call-start = ((), (), s32[]{:S(2)}) async-start(), calls=%async_computation.4 | async-start | bytes 2228224 | tf_op jit(solution)/shard_map/all_gather | solution.py:51
  7.9 143.3 %all-gather.6.cloned.1.call-start = ((), (), s32[]{:S(2)}) async-start(), calls=%async_computation.2 | async-start | bytes 4456448 | tf_op jit(solution)/shard_map/all_gather | solution.py:50
  8.7 240.9 %reduce-scatter.5.cloned.1.call-start = ((), (), s32[]{:S(2)}) async-start(), calls=%async_computation.5 | async-start | bytes 4456448 | tf_op jit(solution)/shard_map/reduce_scatter | solution.py:58
  74.0 5.3 %copy-start.1 = (bf16[1024,2048]{1,0:T(8,128)(2,1)S(1)}, bf16[1024,2048]{1,0:T(8,128)(2,1)}, u32[]{:S(2)}) copy-start(bf16[1024,2048]{1,0:T(8,128)(2,1)} %param.15) | copy-start | bytes 12582916
  86.2 244.5 %reduce-scatter.3.cloned.1.call-start = ((), (), s32[]{:S(2)}) async-start(), calls=%async_computation.3 | async-start | bytes 1114112 | tf_op jit(solution)/shard_map/reduce_scatter | solution.py:55
  160.1 89.5 %copy-start.9 = (f32[32,2048]{1,0:T(8,128)S(1)}, f32[32,2048]{1,0:T(8,128)}, u32[]{:S(2)}) copy-start(f32[32,2048]{1,0:T(8,128)} %param.23) | copy-start | bytes 786436
  160.1 89.5 %copy-start.10 = (f32[32,2048]{1,0:T(8,128)S(1)}, f32[32,2048]{1,0:T(8,128)}, u32[]{:S(2)}) copy-start(f32[32,2048]{1,0:T(8,128)} %param.22) | copy-start | bytes 786436
  161.8 89.5 %copy-start.6 = (f32[256,512]{1,0:T(8,128)S(1)}, f32[256,512]{1,0:T(8,128)}, u32[]{:S(2)}) copy-start(f32[256,512]{1,0:T(8,128)} %param.16) | copy-start | bytes 1572868
  161.8 168.8 %copy-start.11 = (f32[32,512]{1,0:T(8,128)S(1)}, f32[32,512]{1,0:T(8,128)}, u32[]{:S(2)}) copy-start(f32[32,512]{1,0:T(8,128)} %param.21) | copy-start | bytes 196612
  161.8 168.8 %copy-start.12 = (f32[32,512]{1,0:T(8,128)S(1)}, f32[32,512]{1,0:T(8,128)}, u32[]{:S(2)}) copy-start(f32[32,512]{1,0:T(8,128)} %param.20) | copy-start | bytes 196612
  161.8 253.3 %copy-start.2 = (bf16[256,512]{1,0:T(8,128)(2,1)S(1)}, bf16[256,512]{1,0:T(8,128)(2,1)}, u32[]{:S(2)}) copy-start(bf16[256,512]{1,0:T(8,128)(2,1)} %param.18) | copy-start | bytes 786436
  161.9 256.9 %all-gather.10.cloned.1.call-start = ((), (), s32[]{:S(2)}) async-start(), calls=%async_computation.6 | async-start | bytes 2228224 | tf_op jit(solution)/shard_map/all_gather | solution.py:75
  251.3 165.2 %copy-start.3 = (f32[32,2048]{1,0:T(8,128)}, f32[32,2048]{1,0:T(8,128)S(1)}, u32[]{:S(2)}) copy-start(f32[32,2048]{1,0:T(8,128)S(1)} %get-tuple-element.19) | copy-start | bytes 786436
  251.3 165.2 %copy-start.4 = (f32[32,2048]{1,0:T(8,128)}, f32[32,2048]{1,0:T(8,128)S(1)}, u32[]{:S(2)}) copy-start(f32[32,2048]{1,0:T(8,128)S(1)} %get-tuple-element.20) | copy-start | bytes 786436
  251.3 196.5 %all-gather.12.cloned.1.call-start = ((), (), s32[]{:S(2)}) async-start(), calls=%async_computation.7 | async-start | bytes 1310720 | tf_op jit(solution)/shard_map/all_gather | solution.py:81
  332.1 0.6 copy-start.7
  332.1 0.6 copy-start.8
  415.2 3.6 copy-start.5
  416.4 78.1 %all-gather.14.cloned.1.call-start = ((), (), s32[]{:S(2)}) async-start(), calls=%async_computation.8 | async-start | bytes 2621440 | tf_op jit(solution)/shard_map/all_gather | solution.py:84
Sparse Core Ops, SparseCore 0:
  10.8 63.1 all-gather.7
  76.8 74.3 all-gather.5
  153.5 96.0 reduce-scatter.4
  252.2 78.3 reduce-scatter.2
  333.9 58.0 all-gather.9
  416.6 31.1 all-gather.11
  449.9 44.5 all-gather.13
where the time goes:
time: 506 us; the launch traced here: 505 us
  waiting for transfers between devices  365 us (72%)
  blocking collectives  81 us (16%)
  matrix products  27.1 us (5%)
  between operations  15.7 us (3%)
  local copies, waits for them, and re-layouts  12 us (2%)
    reduce_scatter x1, waiting for transfers between devices, body(): lax.psum_scatter(split_rows(output_inner, layer_cotangent), ('rep', 'fs')...  87.6 us
    reduce_scatter x1, waiting for transfers between devices, body(): lax.psum_scatter(split_rows(query_inner, query_cotangent), ('rep', 'fs'),...  79.1 us
    all_gather x1, waiting for transfers between devices, body(): lax.all_gather(output_basis, ('rep', 'fs'), axis=0, tiled=True)  65.3 us
    all_gather x1, waiting for transfers between devices, body(): lax.all_gather(query_basis, ('rep', 'fs'), axis=0, tiled=True)  65 us
    all_gather x1, blocking collectives, body(): lax.all_gather(normed_q.astype(jnp.bfloat16), ('rep', 'fs'), axis=0, tile...  43.2 us
    all_gather x1, waiting for transfers between devices, body(): lax.all_gather((output_weight - step_rate * update_o).astype(jnp.bfloat16...  43.1 us
    psum x1, blocking collectives, body(): lax.psum((jnp.sum(normed_q * normed_q), jnp.sum(normed_o * normed_o)), ('...  37.8 us
    all_gather x1, waiting for transfers between devices, body(): lax.all_gather((query_weight - step_rate * update_q).astype(jnp.bfloat16)...  23.8 us
  transfers between devices with their start and end apart: 7, of which 6 were waited for; matrix products, arithmetic and copies ran while one was open for 8% of the time, Pallas kernels for 0%

commit v1 on v0

--- a/solution.py
+++ b/solution.py
@@ -61,7 +61,7 @@
     first_q, second_q, normed_q = moments(query_first, query_second, projected_q)
     first_o, second_o, normed_o = moments(output_first, output_second, projected_o)
     totals = lax.psum(
-        (jnp.sum(normed_q * normed_q), jnp.sum(normed_o * normed_o)), ("fs", "rep", "tp")
+        lax.psum((jnp.sum(normed_q * normed_q), jnp.sum(normed_o * normed_o)), ("rep", "tp")), "fs"
     )
     scale_q = lax.rsqrt(totals[0] / (R * QKW) + small_eps)
     scale_o = lax.rsqrt(totals[1] / (R * D) + small_eps)

time: 506 us -> 488 us (0.964)
  blocking collectives: 81 us -> 65.7 us
    psum x1, blocking collectives: 37.8 us -> 13.5 us  [body(): lax.psum((jnp.sum(normed_q * normed_q), jnp.sum(normed_o * normed_o)), ('...]
    psum x0 -> x1, blocking collectives: none -> 8.98 us  [body(): lax.psum(lax.psum((jnp.sum(normed_q * normed_q), jnp.sum(normed_o * norme...]
where the time goes in v1:
time: 488 us; the launch traced here: 487 us
  waiting for transfers between devices  363 us (74%)
  blocking collectives  65.7 us (13%)
  matrix products  27.1 us (6%)
  between operations  15.7 us (3%)
  local copies, waits for them, and re-layouts  12 us (2%)
    reduce_scatter x1, waiting for transfers between devices, body(): lax.psum_scatter(split_rows(output_inner, layer_cotangent), ('rep', 'fs')...  87.6 us
    reduce_scatter x1, waiting for transfers between devices, body(): lax.psum_scatter(split_rows(query_inner, query_cotangent), ('rep', 'fs'),...  79.1 us
    all_gather x1, waiting for transfers between devices, body(): lax.all_gather(output_basis, ('rep', 'fs'), axis=0, tiled=True)  65.3 us
    all_gather x1, waiting for transfers between devices, body(): lax.all_gather(query_basis, ('rep', 'fs'), axis=0, tiled=True)  65 us
    all_gather x1, blocking collectives, body(): lax.all_gather(normed_q.astype(jnp.bfloat16), ('rep', 'fs'), axis=0, tile...  43.2 us
    all_gather x1, waiting for transfers between devices, body(): lax.all_gather((output_weight - step_rate * update_o).astype(jnp.bfloat16...  43.1 us
    all_gather x1, waiting for transfers between devices, body(): lax.all_gather((query_weight - step_rate * update_q).astype(jnp.bfloat16)...  20.9 us
    psum x1, blocking collectives, body(): lax.psum((jnp.sum(normed_q * normed_q), jnp.sum(normed_o * normed_o)), ('...  13.5 us
  transfers between devices with their start and end apart: 7, of which 6 were waited for; matrix products, arithmetic and copies ran while one was open for 8% of the time, Pallas kernels for 0%

profile of v1, /device:TPU:0, one launch (start us, length us, event | category | flops | bytes accessed | tf_op | source)
XLA Modules:
  0.0 487.2 jit_solution(12631001307843496341)
XLA Ops:
  8.7 65.3 %all-gather.8.cloned.1.call-done = bf16[2048,512]{1,0:T(8,128)(2,1)} async-done(((bf16[128,512]{1,0:T(8,128)(2,1)}), bf16[2048,512]{1,0:T(8,128)(2,1)}) %all-gather.8.cloned.1.call-update) | async-done | bytes 2097168 | tf_op jit(solution)/shard_map/all_gather | solution.py:51
  74.0 5.3 %fusion.15 = f32[1024,512]{1,0:T(8,128)S(1)} fusion(bf16[1024,2048]{1,0:T(8,128)(2,1)} %param.14, bf16[2048,512]{1,0:T(8,128)(2,1)} %all-gather.8.cloned.1.call-done), kind=kOutput, calls=%fused_computation.29 | convolution fusion | flops 2147483648 | bytes 8388608 | tf_op jit(solution)/shard_map/dot_general | solution.py:54
  79.4 2.4 fusion.3
  81.7 4.4 convolution_add_fusion
  86.2 65.0 %all-gather.6.cloned.1.call-done = bf16[4096,512]{1,0:T(8,128)(2,1)} async-done(((bf16[256,512]{1,0:T(8,128)(2,1)}), bf16[4096,512]{1,0:T(8,128)(2,1)}) %all-gather.6.cloned.1.call-update) | async-done | bytes 4194320 | tf_op jit(solution)/shard_map/all_gather | solution.py:50
  151.2 8.1 %fusion.14 = f32[1024,512]{1,0:T(8,128)S(1)} fusion(bf16[1024,4096]{1,0:T(8,128)(2,1)} %param.12, bf16[4096,512]{1,0:T(8,128)(2,1)} %all-gather.6.cloned.1.call-done), kind=kOutput, calls=%fused_computation.28 | convolution fusion | flops 4294967296 | bytes 14680064 | tf_op jit(solution)/shard_map/dot_general | solution.py:53
  159.3 0.7 fusion.6
  160.1 1.7 convolution_add_fusion.1
  161.9 87.6 %reduce-scatter.5.cloned.1.call-done = f32[32,2048]{1,0:T(8,128)} async-done(((f32[512,2048]{1,0:T(8,128)}), f32[32,2048]{1,0:T(8,128)}) %reduce-scatter.5.cloned.1.call-update) | async-done | bytes 262160 | tf_op jit(solution)/shard_map/reduce_scatter | solution.py:58
  249.6 1.7 fusion.9
  251.5 79.1 %reduce-scatter.3.cloned.1.call-done = f32[32,512]{1,0:T(8,128)} async-done(((f32[512,512]{1,0:T(8,128)}), f32[32,512]{1,0:T(8,128)}) %reduce-scatter.3.cloned.1.call-update) | async-done | bytes 65552 | tf_op jit(solution)/shard_map/reduce_scatter | solution.py:55
  330.6 1.5 multiply_reduce_fusion.1
  332.8 43.2 %all_gather.19 = bf16[512,512]{1,0:T(8,128)(2,1)S(1)} all-gather(bf16[32,512]{1,0:T(8,128)(2,1)S(1)} %fusion.11), channel_id=1, replica_groups=mesh['fs'=4,'rep'=4,'tp'=2] {'rep','fs'}, dimensions={0}, use_global_device_ids=true | all-gather | bytes 557056 | tf_op jit(solution)/shard_map/all_gather | solution.py:70
  376.7 13.5 %all-reduce = (f32[]{:T(128)}, f32[]{:T(128)}) all-reduce(f32[]{:T(128)} %get-tuple-element.23, f32[]{:T(128)} %multiply_reduce_fusion), channel_id=1, replica_groups=mesh['fs'=4,'rep'=4,'tp'=2] {'rep','tp'}, use_global_device_ids=true, to_apply=%region_2.0 | all-reduce | flops 2 | bytes 16 | tf_op jit(solution)/shard_map/psum | solution.py:64
  390.2 9.0 %all-reduce.1 = (f32[]{:T(128)}, f32[]{:T(128)}) all-reduce(f32[]{:T(128)} %get-tuple-element.16, f32[]{:T(128)} %get-tuple-element.17), channel_id=1, replica_groups=mesh['fs'=4,'rep'=4,'tp'=2] {'fs'}, use_global_device_ids=true, to_apply=%region_3.0 | all-reduce | flops 2 | bytes 16 | tf_op jit(solution)/shard_map/psum | solution.py:63
  399.9 1.2 subtract_convert_fusion.5
  401.2 1.6 copy.21
  403.5 3.1 subtract_convert_fusion.4
  406.7 2.1 copy.22
  408.7 20.9 %all-gather.12.cloned.1.call-done = bf16[1024,512]{0,1:T(8,128)(2,1)} async-done(((bf16[256,512]{0,1:T(8,128)(2,1)}), bf16[1024,512]{0,1:T(8,128)(2,1)}) %all-gather.12.cloned.1.call-update) | async-done | bytes 1048592 | tf_op jit(solution)/shard_map/all_gather | solution.py:81
  429.7 2.3 copy.24
  431.9 1.3 copy.23
  433.3 43.1 %all-gather.14.cloned.1.call-done = bf16[512,2048]{0,1:T(8,128)(2,1)} async-done(((bf16[128,2048]{0,1:T(8,128)(2,1)}), bf16[512,2048]{0,1:T(8,128)(2,1)}) %all-gather.14.cloned.1.call-update) | async-done | bytes 2097168 | tf_op jit(solution)/shard_map/all_gather | solution.py:84
  476.4 3.9 copy.25
  (44 shorter events, 3.4 us)
Async XLA Ops:
  7.2 152.2 %copy-start = (bf16[1024,512]{1,0:T(8,128)(2,1)S(1)}, bf16[1024,512]{1,0:T(8,128)(2,1)}, u32[]{:S(2)}) copy-start(bf16[1024,512]{1,0:T(8,128)(2,1)} %param.13) | copy-start | bytes 3145732
  7.2 66.8 %all-gather.8.cloned.1.call-start = ((), (), s32[]{:S(2)}) async-start(), calls=%async_computation.4 | async-start | bytes 2228224 | tf_op jit(solution)/shard_map/all_gather | solution.py:51
  7.9 143.3 %all-gather.6.cloned.1.call-start = ((), (), s32[]{:S(2)}) async-start(), calls=%async_computation.2 | async-start | bytes 4456448 | tf_op jit(solution)/shard_map/all_gather | solution.py:50
  8.7 240.9 %reduce-scatter.5.cloned.1.call-start = ((), (), s32[]{:S(2)}) async-start(), calls=%async_computation.5 | async-start | bytes 4456448 | tf_op jit(solution)/shard_map/reduce_scatter | solution.py:58
  74.0 5.3 %copy-start.1 = (bf16[1024,2048]{1,0:T(8,128)(2,1)S(1)}, bf16[1024,2048]{1,0:T(8,128)(2,1)}, u32[]{:S(2)}) copy-start(bf16[1024,2048]{1,0:T(8,128)(2,1)} %param.15) | copy-start | bytes 12582916
  86.2 244.5 %reduce-scatter.3.cloned.1.call-start = ((), (), s32[]{:S(2)}) async-start(), calls=%async_computation.3 | async-start | bytes 1114112 | tf_op jit(solution)/shard_map/reduce_scatter | solution.py:55
  160.1 89.5 %copy-start.9 = (f32[32,2048]{1,0:T(8,128)S(1)}, f32[32,2048]{1,0:T(8,128)}, u32[]{:S(2)}) copy-start(f32[32,2048]{1,0:T(8,128)} %param.23) | copy-start | bytes 786436
  160.1 89.5 %copy-start.10 = (f32[32,2048]{1,0:T(8,128)S(1)}, f32[32,2048]{1,0:T(8,128)}, u32[]{:S(2)}) copy-start(f32[32,2048]{1,0:T(8,128)} %param.22) | copy-start | bytes 786436
  161.8 89.5 %copy-start.6 = (f32[256,512]{1,0:T(8,128)S(1)}, f32[256,512]{1,0:T(8,128)}, u32[]{:S(2)}) copy-start(f32[256,512]{1,0:T(8,128)} %param.16) | copy-start | bytes 1572868
  161.8 168.8 %copy-start.11 = (f32[32,512]{1,0:T(8,128)S(1)}, f32[32,512]{1,0:T(8,128)}, u32[]{:S(2)}) copy-start(f32[32,512]{1,0:T(8,128)} %param.21) | copy-start | bytes 196612
  161.8 168.8 %copy-start.12 = (f32[32,512]{1,0:T(8,128)S(1)}, f32[32,512]{1,0:T(8,128)}, u32[]{:S(2)}) copy-start(f32[32,512]{1,0:T(8,128)} %param.20) | copy-start | bytes 196612
  161.8 238.1 %copy-start.2 = (bf16[256,512]{1,0:T(8,128)(2,1)S(1)}, bf16[256,512]{1,0:T(8,128)(2,1)}, u32[]{:S(2)}) copy-start(bf16[256,512]{1,0:T(8,128)(2,1)} %param.18) | copy-start | bytes 786436
  161.9 241.6 %all-gather.10.cloned.1.call-start = ((), (), s32[]{:S(2)}) async-start(), calls=%async_computation.6 | async-start | bytes 2228224 | tf_op jit(solution)/shard_map/all_gather | solution.py:75
  251.3 149.9 %copy-start.3 = (f32[32,2048]{1,0:T(8,128)}, f32[32,2048]{1,0:T(8,128)S(1)}, u32[]{:S(2)}) copy-start(f32[32,2048]{1,0:T(8,128)S(1)} %get-tuple-element.21) | copy-start | bytes 786436
  251.3 149.9 %copy-start.4 = (f32[32,2048]{1,0:T(8,128)}, f32[32,2048]{1,0:T(8,128)S(1)}, u32[]{:S(2)}) copy-start(f32[32,2048]{1,0:T(8,128)S(1)} %get-tuple-element.22) | copy-start | bytes 786436
  251.3 178.4 %all-gather.12.cloned.1.call-start = ((), (), s32[]{:S(2)}) async-start(), calls=%async_computation.7 | async-start | bytes 1310720 | tf_op jit(solution)/shard_map/all_gather | solution.py:81
  332.1 0.6 copy-start.7
  332.1 0.6 copy-start.8
  399.9 3.6 copy-start.5
  401.2 75.2 %all-gather.14.cloned.1.call-start = ((), (), s32[]{:S(2)}) async-start(), calls=%async_computation.8 | async-start | bytes 2621440 | tf_op jit(solution)/shard_map/all_gather | solution.py:84
Sparse Core Ops, SparseCore 0:
  10.8 63.1 all-gather.7
  76.8 74.3 all-gather.5
  153.5 96.0 reduce-scatter.4
  252.2 78.3 reduce-scatter.2
  333.9 57.8 all-gather.9
  401.3 28.3 all-gather.11
  431.8 44.5 all-gather.13
